TPU v7x, 512 devices: a whole 4x8x8 slice. The times are simulated.
512 devices in a mesh: kv: 64 (over z, y), tp: 8 (over x, core).
Axes of the slice: x: 4, y: 8, z: 8, core: 2. Of those that a mesh axis runs over, the one named last changes fastest.
Arguments:
- tokens: bfloat16 [8, 8192, 2048], P(None, 'kv'), may hold values from -32 to 32, as said below
- w_query: bfloat16 [2048, 1024], P(None, 'tp'), may hold values from -0.125 to 0.125
- w_key: bfloat16 [2048, 512], P(None, 'tp'), may hold values from -0.125 to 0.125
- w_value: bfloat16 [2048, 512], P(None, 'tp'), may hold values from -0.125 to 0.125
- w_output: bfloat16 [1024, 2048], P(None, 'tp'), may hold values from -3 to 3
- chosen: int32 [8, 64, 32], P(None, 'kv'), may hold values from -1 to 63, as said below
- lengths: int32 [8], replicated, may hold values from 1 to 8192, 22528 in all
Outputs:
- mixed: bfloat16 [8, 8192, 2048], P(None, 'kv', 'tp')
Inputs may be any that keep to these rules, and one draw needn't show every extreme that they name: chosen[s, b] lists distinct blocks of sequence s, none above b; its first entry is b; entries after the named ones are -1. For b >= 1 and each c < b, at most 4 of the 8 lists chosen[:, b] name block c, and exactly 4 of them name block b - 1. lengths[s] is the number of live positions of sequence s; the largest is 8192. `tokens`: activations of order one; some rows may be much larger.
All inputs are finite; a program needn't handle non-finite values.
Results may differ from a plain program's by a relative error of at most 0.012.
The roundings to bfloat16 on the way count: a program that leaves them out, or rounds other values in their place, can miss the bound.
Values may be sent and summed in bfloat16 or wider, within the bound.
A program may use at most 128 MiB of HBM per device.

v0:
```python
import jax
import jax.numpy as jnp
from jax import lax
from jax.sharding import PartitionSpec as P

HEADS = 16
KV_HEADS = 8
HEAD_DIM = 64


def per_device(tokens, w_query, w_key, w_value, w_output, chosen, lengths):
    seq_count, block_len, model_width = tokens.shape
    flat_rows = tokens.reshape(seq_count * block_len, model_width)
    queries = jnp.dot(flat_rows, w_query, preferred_element_type=jnp.float32).astype(jnp.bfloat16)
    key_proj = jnp.dot(flat_rows, w_key, preferred_element_type=jnp.float32).astype(jnp.bfloat16)
    value_proj = jnp.dot(flat_rows, w_value, preferred_element_type=jnp.float32).astype(
        jnp.bfloat16
    )
    key_width = key_proj.shape[1]
    local_blocks = jnp.concatenate([key_proj, value_proj], axis=1).reshape(
        seq_count, block_len, 2 * key_width
    )
    shard_member = lax.axis_index("kv")
    kv_devices = lax.axis_size("kv")
    picked = chosen[:, 0, :]
    clipped = jnp.maximum(picked, 0)
    seq_index = jnp.arange(seq_count, dtype=jnp.int32)
    gathered = lax.all_gather(local_blocks, "kv", axis=1, tiled=True)
    key_lookup = gathered.reshape(seq_count * kv_devices, block_len, 2 * key_width)
    source = seq_index[:, None] * kv_devices + clipped
    group_size = HEADS // KV_HEADS
    local_kv_heads = key_width // HEAD_DIM
    query_pos = shard_member * block_len + jnp.arange(block_len, dtype=jnp.int32)
    score_scale = HEAD_DIM ** (-0.5)

    def attend(packed):
        query_rows, source_row, pick_row, length = packed
        fetched = key_lookup[source_row]
        slot_count = pick_row.shape[0]
        key_rows = fetched[:, :, :key_width].reshape(
            slot_count * block_len, local_kv_heads, HEAD_DIM
        )
        value_rows = fetched[:, :, key_width:].reshape(
            slot_count * block_len, local_kv_heads, HEAD_DIM
        )
        grouped = query_rows.reshape(block_len, local_kv_heads, group_size, HEAD_DIM)
        scores = (
            jnp.einsum("qkgd,nkd->kgqn", grouped, key_rows, preferred_element_type=jnp.float32)
            * score_scale
        )
        key_pos = (
            pick_row[:, None] * block_len + jnp.arange(block_len, dtype=jnp.int32)[None, :]
        ).reshape(-1)
        listed = jnp.repeat(pick_row >= 0, block_len)
        allowed = (
            listed[None, :] & (key_pos[None, :] <= query_pos[:, None]) & (key_pos[None, :] < length)
        )
        masked = jnp.where(allowed, scores, -1e30)
        row_max = jnp.max(masked, axis=-1, keepdims=True)
        exponent = jnp.exp(masked - row_max)
        weights = (exponent / jnp.sum(exponent, axis=-1, keepdims=True)).astype(jnp.bfloat16)
        mixed_heads = jnp.einsum(
            "kgqn,nkd->qkgd", weights, value_rows, preferred_element_type=jnp.float32
        )
        live_rows = (query_pos < length)[:, None, None, None]
        return jnp.where(live_rows, mixed_heads, 0.0).astype(jnp.bfloat16).reshape(block_len, -1)

    attended = lax.map(attend, (queries.reshape(seq_count, block_len, -1), source, picked, lengths))
    attended_rows = attended.reshape(seq_count * block_len, -1)
    summed = jnp.dot(
        lax.all_gather(attended_rows, "tp", axis=1, tiled=True),
        w_output,
        preferred_element_type=jnp.float32,
    )
    return summed.astype(jnp.bfloat16).reshape(seq_count, block_len, -1)


def solution(mesh):
    return jax.shard_map(
        per_device,
        mesh=mesh,
        in_specs=(
            P(None, "kv", None),
            P(None, "tp"),
            P(None, "tp"),
            P(None, "tp"),
            P(None, "tp"),
            P(None, "kv", None),
            P(),
        ),
        out_specs=P(None, "kv", "tp"),
        check_vma=False,
    )
```

profile of v0, /device:TPU:1, one launch (start us, length us, event | category | flops | bytes accessed | tf_op | source)
XLA Modules:
  0.0 374.0 jit_solution(2250813190140114071)
XLA Ops:
  6.5 3.8 %convolution_convert_fusion.2 = bf16[1024,64]{0,1:T(8,128)(2,1)S(1)} fusion(bf16[1024,2048]{1,0:T(8,128)(2,1)} %bitcast.109, bf16[2048,64]{0,1:T(8,128)(2,1)} %param.12), kind=kOutput, calls=%fused_computation.31 | convolution fusion | flops 268500992 | bytes 4587520 | tf_op jit(solution)/shard_map/dot_general | solution.py:16
  10.3 1.4 convolution_convert_fusion.3
  12.7 4.2 %convolution_convert_fusion.1 = bf16[1024,128]{1,0:T(8,128)(2,1)} fusion(bf16[1024,2048]{1,0:T(8,128)(2,1)} %bitcast.110, bf16[2048,128]{1,0:T(8,128)(2,1)S(1)} %copy-done.5), kind=kOutput, calls=%fused_computation.30 | convolution fusion | flops 537001984 | bytes 4980736 | tf_op jit(solution)/shard_map/dot_general | solution.py:14
  16.9 144.8 %all-gather.3.cloned.1.call-done = bf16[8,8192,128]{1,0,2:T(8,128)(2,1)} async-done(((bf16[8,128,128]{1,0,2:T(8,128)(2,1)}), bf16[8,8192,128]{1,0,2:T(8,128)(2,1)}) %all-gather.3.cloned.1.call-update) | async-done | bytes 16777232 | tf_op jit(solution)/shard_map/all_gather | solution.py:28
  161.7 23.5 %copy.16 = bf16[8,8192,128]{2,1,0:T(8,128)(2,1)} copy(bf16[8,8192,128]{1,0,2:T(8,128)(2,1)} %all-gather.3.cloned.1.call-done) | data formatting | bytes 33554432 | tf_op jit(solution)/shard_map/all_gather | solution.py:28
  185.2 145.3 %while.11 = (s32[]{:T(128)}, bf16[8,128,128]{2,1,0:T(8,128)(2,1)S(1)}, s32[8]{0:T(128)S(1)}, s32[8,32]{1,0:T(8,128)S(1)}, bf16[512,128,128]{2,1,0:T(8,128)(2,1)}...) while((s32[]{:T(128)}, bf16[8,128,128]{2,1,0:T(8,128)(2,1)S(1)}, ...), condition=%wide.region_3.4_spmd.clone, body=%wide.region_0.3_spmd.clone.sunk | while | flops 278443040 | bytes 19263052 | solution.py:68
  186.7 3.5 and_and_fusion.2
  190.2 6.5 %gather_fusion = bf16[32,128,128]{2,1,0:T(8,128)(2,1)S(1)} fusion(bf16[512,128,128]{2,1,0:T(8,128)(2,1)} %get-tuple-element.182, s32[1024]{0:T(1024)S(1)} %pad_clamp_fusion.2), kind=kCustom, calls=%fused_computation.clone.clone.1 | custom fusion | bytes 2097280 | tf_op jit(solution)/shard_map/while/body/eval_jaxpr/gather | solution.py:38
  196.7 1.4 fusion.45
  199.1 2.1 fusion.46
  202.4 0.9 fusion.48
  204.9 3.5 and_and_fusion.2
  208.4 6.5 %gather_fusion = bf16[32,128,128]{2,1,0:T(8,128)(2,1)S(1)} fusion(bf16[512,128,128]{2,1,0:T(8,128)(2,1)} %get-tuple-element.182, s32[1024]{0:T(1024)S(1)} %pad_clamp_fusion.2), kind=kCustom, calls=%fused_computation.clone.clone.1 | custom fusion | bytes 2097280 | tf_op jit(solution)/shard_map/while/body/eval_jaxpr/gather | solution.py:38
  214.9 1.4 fusion.45
  217.2 2.1 fusion.46
  220.5 0.9 fusion.48
  223.0 3.5 and_and_fusion.2
  226.6 6.5 %gather_fusion = bf16[32,128,128]{2,1,0:T(8,128)(2,1)S(1)} fusion(bf16[512,128,128]{2,1,0:T(8,128)(2,1)} %get-tuple-element.182, s32[1024]{0:T(1024)S(1)} %pad_clamp_fusion.2), kind=kCustom, calls=%fused_computation.clone.clone.1 | custom fusion | bytes 2097280 | tf_op jit(solution)/shard_map/while/body/eval_jaxpr/gather | solution.py:38
  233.1 1.4 fusion.45
  235.4 2.1 fusion.46
  238.7 0.9 fusion.48
  241.2 3.5 and_and_fusion.2
  244.7 6.5 %gather_fusion = bf16[32,128,128]{2,1,0:T(8,128)(2,1)S(1)} fusion(bf16[512,128,128]{2,1,0:T(8,128)(2,1)} %get-tuple-element.182, s32[1024]{0:T(1024)S(1)} %pad_clamp_fusion.2), kind=kCustom, calls=%fused_computation.clone.clone.1 | custom fusion | bytes 2097280 | tf_op jit(solution)/shard_map/while/body/eval_jaxpr/gather | solution.py:38
  251.2 1.4 fusion.45
  253.6 2.1 fusion.46
  256.9 0.9 fusion.48
  259.4 3.5 and_and_fusion.2
  262.9 6.5 %gather_fusion = bf16[32,128,128]{2,1,0:T(8,128)(2,1)S(1)} fusion(bf16[512,128,128]{2,1,0:T(8,128)(2,1)} %get-tuple-element.182, s32[1024]{0:T(1024)S(1)} %pad_clamp_fusion.2), kind=kCustom, calls=%fused_computation.clone.clone.1 | custom fusion | bytes 2097280 | tf_op jit(solution)/shard_map/while/body/eval_jaxpr/gather | solution.py:38
  269.4 1.4 fusion.45
  271.7 2.1 fusion.46
  275.0 0.9 fusion.48
  277.5 3.5 and_and_fusion.2
  281.1 6.5 %gather_fusion = bf16[32,128,128]{2,1,0:T(8,128)(2,1)S(1)} fusion(bf16[512,128,128]{2,1,0:T(8,128)(2,1)} %get-tuple-element.182, s32[1024]{0:T(1024)S(1)} %pad_clamp_fusion.2), kind=kCustom, calls=%fused_computation.clone.clone.1 | custom fusion | bytes 2097280 | tf_op jit(solution)/shard_map/while/body/eval_jaxpr/gather | solution.py:38
  287.6 1.4 fusion.45
  289.9 2.1 fusion.46
  293.2 0.9 fusion.48
  295.7 3.5 and_and_fusion.2
  299.2 6.5 %gather_fusion = bf16[32,128,128]{2,1,0:T(8,128)(2,1)S(1)} fusion(bf16[512,128,128]{2,1,0:T(8,128)(2,1)} %get-tuple-element.182, s32[1024]{0:T(1024)S(1)} %pad_clamp_fusion.2), kind=kCustom, calls=%fused_computation.clone.clone.1 | custom fusion | bytes 2097280 | tf_op jit(solution)/shard_map/while/body/eval_jaxpr/gather | solution.py:38
  305.8 1.4 fusion.45
  308.1 2.1 fusion.46
  311.4 0.9 fusion.48
  313.9 3.5 and_and_fusion.2
  317.4 6.5 %gather_fusion = bf16[32,128,128]{2,1,0:T(8,128)(2,1)S(1)} fusion(bf16[512,128,128]{2,1,0:T(8,128)(2,1)} %get-tuple-element.182, s32[1024]{0:T(1024)S(1)} %pad_clamp_fusion.2), kind=kCustom, calls=%fused_computation.clone.clone.1 | custom fusion | bytes 2097280 | tf_op jit(solution)/shard_map/while/body/eval_jaxpr/gather | solution.py:38
  323.9 1.4 fusion.45
  326.2 2.1 fusion.46
  329.5 0.9 fusion.48
  331.3 32.8 %all-gather.5.cloned.1.call-done = bf16[1024,1024]{1,0:T(8,128)(2,1)} async-done(((bf16[1024,128]{1,0:T(8,128)(2,1)}), bf16[1024,1024]{1,0:T(8,128)(2,1)}) %all-gather.5.cloned.1.call-update) | async-done | bytes 2097168 | tf_op jit(solution)/shard_map/all_gather | solution.py:71
  364.1 3.1 convolution_convert_fusion
  (143 shorter events, 31.3 us)
Async XLA Ops:
  6.5 357.5 %copy-start = (bf16[1024,256]{1,0:T(8,128)(2,1)S(1)}, bf16[1024,256]{1,0:T(8,128)(2,1)}, u32[]{:S(2)}) copy-start(bf16[1024,256]{1,0:T(8,128)(2,1)} %param.13) | copy-start | bytes 1572868
  6.5 3.8 %copy-start.2 = (bf16[2048,64]{0,1:T(8,128)(2,1)S(1)}, bf16[2048,64]{0,1:T(8,128)(2,1)}, u32[]{:S(2)}) copy-start(bf16[2048,64]{0,1:T(8,128)(2,1)} %param.11) | copy-start | bytes 786436
  6.5 155.2 %all-gather.3.cloned.1.call-start = ((), (), s32[]{:S(2)}) async-start(), calls=%async_computation | async-start | bytes 17039360 | tf_op jit(solution)/shard_map/all_gather | solution.py:28
  6.5 3.8 %copy-start.1 = (bf16[8,128,2048]{2,1,0:T(8,128)(2,1)S(1)}, bf16[8,128,2048]{2,1,0:T(8,128)(2,1)}, u32[]{:S(2)}) copy-start(bf16[8,128,2048]{2,1,0:T(8,128)(2,1)} %param.9) | copy-start | bytes 12582916
  10.3 2.3 copy-start.4
  10.3 2.4 copy-start.5
  12.5 351.5 %all-gather.5.cloned.1.call-start = ((), (), s32[]{:S(2)}) async-start(), calls=%async_computation.1 | async-start | bytes 2359296 | tf_op jit(solution)/shard_map/all_gather | solution.py:71
  16.9 168.4 %copy-start.6 = (s32[8]{0:T(128)S(1)}, s32[8]{0:T(128)}, u32[]{:S(2)}) copy-start(s32[8]{0:T(128)} %param.15) | copy-start | bytes 100
  330.6 0.7 copy-start.3
Sparse Core Ops, SparseCore 0:
  12.7 148.9 all-gather.2
  331.4 32.6 all-gather.4
where the time goes:
time: 376 us; the launch traced here: 374 us
  waiting for transfers between devices  178 us (47%)
  local copies, waits for them, and re-layouts  102 us (27%)
  other arithmetic  44.2 us (12%)
  matrix products  36 us (10%)
  between operations  13.5 us (4%)
    all_gather x1, waiting for transfers between devices, per_device(): gathered = lax.all_gather(local_blocks, 'kv', axis=1, tiled=True)  145 us
    gather x8, local copies, waits for them, and re-layouts, attend(): fetched = key_lookup[source_row]  52.1 us
    all_gather x1, waiting for transfers between devices, per_device(): lax.all_gather(attended_rows, 'tp', axis=1, tiled=True)  32.8 us
    and x8, other arithmetic, attend(): listed[None, :] & (key_pos[None, :] <= query_pos[:, None])  27.7 us
    all_gather x1, local copies, waits for them, and re-layouts, per_device(): gathered = lax.all_gather(local_blocks, 'kv', axis=1, tiled=True)  23.5 us
    dot_general x8, matrix products, attend(): jnp.einsum('qkgd,nkd->kgqn', grouped, key_rows, preferred_element_type=jn...  16.5 us
    dynamic_slice x24, local copies, waits for them, and re-layouts, per_device(): lax.map(attend, (queries.reshape(seq_count, block_len, -1), source, picke...  11.7 us
    slice x8, local copies, waits for them, and re-layouts, attend(): fetched[:, :, :key_width]  11.5 us
  transfers between devices with their start and end apart: 2, of which 2 were waited for; matrix products, arithmetic and copies ran while one was open for 1% of the time, Pallas kernels for 0%

commit v1 on v0

--- a/solution.py
+++ b/solution.py
@@ -25,7 +25,8 @@
     picked = chosen[:, 0, :]
     clipped = jnp.maximum(picked, 0)
     seq_index = jnp.arange(seq_count, dtype=jnp.int32)
-    gathered = lax.all_gather(local_blocks, "kv", axis=1, tiled=True)
+    copies = jnp.concatenate([local_blocks] * lax.axis_size("kv"), axis=1)
+    gathered = lax.all_to_all(copies, "kv", 1, 1, tiled=True)
     key_lookup = gathered.reshape(seq_count * kv_devices, block_len, 2 * key_width)
     source = seq_index[:, None] * kv_devices + clipped
     group_size = HEADS // KV_HEADS

time: 376 us -> 935 us (2.49)
  waiting for transfers between devices: 178 us -> 680 us
  local copies, waits for them, and re-layouts: 102 us -> 139 us
  starting transfers between devices: 0.04 us -> 17.6 us
    all_to_all x0 -> x1, waiting for transfers between devices: none -> 559 us  [per_device(): gathered = lax.all_to_all(copies, 'kv', 1, 1, tiled=True)]
    all_gather x1 -> x0, waiting for transfers between devices: 145 us -> none  [per_device(): gathered = lax.all_gather(local_blocks, 'kv', axis=1, tiled=True)]
    all_gather x1, waiting for transfers between devices: 32.8 us -> 121 us  [per_device(): lax.all_gather(attended_rows, 'tp', axis=1, tiled=True)]
    unnamed x15 -> x74, local copies, waits for them, and re-layouts: 1.48 us -> 46 us
    all_gather x1 -> x0, local copies, waits for them, and re-layouts: 23.5 us -> none  [per_device(): gathered = lax.all_gather(local_blocks, 'kv', axis=1, tiled=True)]
    all_to_all x0 -> x1, starting transfers between devices: none -> 17.5 us  [per_device(): gathered = lax.all_to_all(copies, 'kv', 1, 1, tiled=True)]
    all_to_all x0 -> x1, local copies, waits for them, and re-layouts: none -> 15.1 us  [per_device(): gathered = lax.all_to_all(copies, 'kv', 1, 1, tiled=True)]
  transfers between devices with their start and end apart: 2 -> 2, of which waited for: 2 -> 2; matrix products, arithmetic and copies ran while one was open for 1% -> 0% of each run, Pallas kernels for 0% -> 0%
where the time goes in v1:
time: 935 us; the launch traced here: 933 us
  waiting for transfers between devices  680 us (73%)
  local copies, waits for them, and re-layouts  139 us (15%)
  other arithmetic  43.9 us (5%)
  matrix products  38.1 us (4%)
  starting transfers between devices  17.6 us (2%)
  between operations  13.5 us (1%)
    all_to_all x1, waiting for transfers between devices, per_device(): gathered = lax.all_to_all(copies, 'kv', 1, 1, tiled=True)  559 us
    all_gather x1, waiting for transfers between devices, per_device(): lax.all_gather(attended_rows, 'tp', axis=1, tiled=True)  121 us
    gather x8, local copies, waits for them, and re-layouts, attend(): fetched = key_lookup[source_row]  52.1 us
    unnamed x74, local copies, waits for them, and re-layouts  46 us
    and x8, other arithmetic, attend(): listed[None, :] & (key_pos[None, :] <= query_pos[:, None])  27.7 us
  transfers between devices with their start and end apart: 2, of which 2 were waited for; matrix products, arithmetic and copies ran while one was open for 0% of the time, Pallas kernels for 0%

profile of v1, /device:TPU:1, one launch (start us, length us, event | category | flops | bytes accessed | tf_op | source)
XLA Modules:
  0.0 933.3 jit_solution(9824947096596880113)
XLA Ops:
  6.5 3.7 convolution_convert_fusion.2
  10.2 3.6 convolution_convert_fusion.3
  60.2 17.5 %all-to-all-start = ((bf16[8,8192,128]{2,0,1:T(8,128)(2,1)}), bf16[8,8192,128]{2,0,1:T(8,128)(2,1)}, u32[]{:S(2)}, u32[]{:S(2)}) async-start(bf16[8,8192,128]{2,0,1:T(8,128)(2,1)} %constant_dynamic-update-slice_fusion.1), calls=%async_computation | async-start | bytes 33554432 | tf_op jit(solution)/shard_map/all_to_all | solution.py:29
  77.8 4.1 convolution_convert_fusion.1
  82.0 559.3 %all-to-all-done = bf16[8,8192,128]{2,0,1:T(8,128)(2,1)} async-done(((bf16[8,8192,128]{2,0,1:T(8,128)(2,1)}), bf16[8,8192,128]{2,0,1:T(8,128)(2,1)}, u32[]{:S(2)}, u32[]{:S(2)}) %all-to-all-start) | async-done | bytes 16777248 | tf_op jit(solution)/shard_map/all_to_all | solution.py:29
  641.3 15.1 %copy.296 = bf16[8,8192,128]{2,1,0:T(8,128)(2,1)} copy(bf16[8,8192,128]{2,0,1:T(8,128)(2,1)} %all-to-all-done) | data formatting | bytes 33554432 | tf_op jit(solution)/shard_map/all_to_all | solution.py:29
  656.3 145.1 %while.11 = (s32[]{:T(128)}, bf16[8,128,128]{2,1,0:T(8,128)(2,1)S(1)}, s32[8]{0:T(128)S(1)}, s32[8,32]{1,0:T(8,128)S(1)}, bf16[512,128,128]{2,1,0:T(8,128)(2,1)}...) while((s32[]{:T(128)}, bf16[8,128,128]{2,1,0:T(8,128)(2,1)S(1)}, ...), condition=%wide.region_3.4_spmd.clone, body=%wide.region_0.3_spmd.clone.sunk | while | flops 278443040 | bytes 19263052 | solution.py:69
  657.8 3.5 and_and_fusion.2
  661.3 6.5 gather_fusion
  667.8 1.4 fusion.45
  670.1 2.1 fusion.46
  675.9 3.5 and_and_fusion.2
  679.4 6.5 gather_fusion
  686.0 1.4 fusion.45
  688.3 2.1 fusion.46
  691.6 0.9 fusion.48
  694.1 3.5 and_and_fusion.2
  697.6 6.5 gather_fusion
  704.1 1.4 fusion.45
  706.4 2.1 fusion.46
  709.7 0.9 fusion.48
  712.2 3.5 and_and_fusion.2
  715.7 6.5 gather_fusion
  722.3 1.4 fusion.45
  724.6 2.1 fusion.46
  727.8 0.9 fusion.48
  730.4 3.5 and_and_fusion.2
  733.9 6.5 gather_fusion
  740.4 1.4 fusion.45
  742.7 2.1 fusion.46
  746.0 0.9 fusion.48
  748.5 3.5 and_and_fusion.2
  752.0 6.5 gather_fusion
  758.5 1.4 fusion.45
  760.8 2.1 fusion.46
  764.1 0.9 fusion.48
  766.6 3.5 and_and_fusion.2
  770.1 6.5 gather_fusion
  776.7 1.4 fusion.45
  779.0 2.1 fusion.46
  782.2 0.9 fusion.48
  784.8 3.5 and_and_fusion.2
  788.3 6.5 gather_fusion
  794.8 1.4 fusion.45
  797.1 2.1 fusion.46
  800.4 0.9 fusion.48
  802.1 121.2 %all-gather.2.cloned.1.call-done = bf16[1024,1024]{1,0:T(8,128)(2,1)} async-done(((bf16[1024,128]{1,0:T(8,128)(2,1)}), bf16[1024,1024]{1,0:T(8,128)(2,1)}) %all-gather.2.cloned.1.call-update) | async-done | bytes 2097168 | tf_op jit(solution)/shard_map/all_gather | solution.py:72
  923.3 3.1 convolution_convert_fusion
  (203 shorter events, 77.6 us)
Async XLA Ops:
  6.5 916.8 %copy-start = (bf16[1024,256]{1,0:T(8,128)(2,1)S(1)}, bf16[1024,256]{1,0:T(8,128)(2,1)}, u32[]{:S(2)}) copy-start(bf16[1024,256]{1,0:T(8,128)(2,1)} %param.13) | copy-start | bytes 1572868
  60.1 17.6 %copy-start.2 = (s32[8,1,32]{2,1,0:T(1,128)S(1)}, s32[8,1,32]{2,1,0:T(1,128)}, u32[]{:S(2)}) copy-start(s32[8,1,32]{2,1,0:T(1,128)} %param.14) | copy-start | bytes 3076
  60.1 17.7 %copy-start.3 = (bf16[2048,128]{1,0:T(8,128)(2,1)S(1)}, bf16[2048,128]{1,0:T(8,128)(2,1)}, u32[]{:S(2)}) copy-start(bf16[2048,128]{1,0:T(8,128)(2,1)} %param.10) | copy-start | bytes 1572868
  60.2 581.1 %all-to-all-start = ((bf16[8,8192,128]{2,0,1:T(8,128)(2,1)}), bf16[8,8192,128]{2,0,1:T(8,128)(2,1)}, u32[]{:S(2)}, u32[]{:S(2)}) async-start(bf16[8,8192,128]{2,0,1:T(8,128)(2,1)} %constant_dynamic-update-slice_fusion.1), calls=%async_computation | async-start | bytes 33554432 | tf_op jit(solution)/shard_map/all_to_all | solution.py:29
  77.7 845.6 %all-gather.2.cloned.1.call-start = ((), (), s32[]{:S(2)}) async-start(), calls=%async_computation.1 | async-start | bytes 2359296 | tf_op jit(solution)/shard_map/all_gather | solution.py:72
  82.0 574.3 %copy-start.4 = (s32[8]{0:T(128)S(1)}, s32[8]{0:T(128)}, u32[]{:S(2)}) copy-start(s32[8]{0:T(128)} %param.15) | copy-start | bytes 100
  801.4 0.7 copy-start.1
Sparse Core Ops, SparseCore 0:
  802.3 120.9 all-gather.1
